TPU v7x, 256 devices: a 2x2x32 block of a 4x8x32 slice. The times are simulated.
256 devices in a mesh: grp: 4 (over y, x), ep: 64 (over z, core).
Axes of the slice: x: 2, y: 2, z: 32, core: 2. Of those that a mesh axis runs over, the one named last changes fastest.
The devices are a block of a 4x8x32 slice.
Arguments:
- tokens: bfloat16 [2048, 2048], P(('grp', 'ep')), parts along dimension 0, may hold values from -6 to 6
- first_gain: bfloat16 [2048], replicated, may hold values from 0.099609375 to 1.8984375
- query_weight: bfloat16 [2048, 1024], P(None, 'ep'), may hold values from -0.125 to 0.125
- key_weight: bfloat16 [2048, 1024], P(None, 'ep'), may hold values from -0.125 to 0.125
- value_weight: bfloat16 [2048, 1024], P(None, 'ep'), may hold values from -0.125 to 0.125
- outgate_weight: bfloat16 [2048, 1024], P(None, 'ep'), may hold values from -0.125 to 0.125
- igate_weight: bfloat16 [2048, 8], replicated, may hold values from -0.125 to 0.125
- fgate_weight: bfloat16 [2048, 8], replicated, may hold values from -0.125 to 0.125
- igate_bias: float32 [8], replicated, may hold values from -2 to 1
- fgate_bias: float32 [8], replicated, may hold values from -1 to 4
- memory_state: float32 [2048, 8, 128, 128], P(('grp', 'ep')), parts along dimension 0, may hold values from -0.6 to 0.6
- norm_state: float32 [2048, 8, 128], P(('grp', 'ep')), parts along dimension 0, may hold values from -0.6 to 0.6
- max_state: float32 [2048, 8], P(('grp', 'ep')), parts along dimension 0, may hold values from -1 to 2
- head_gain: bfloat16 [1024], replicated, may hold values from 0.099609375 to 1.8984375
- out_weight: bfloat16 [1024, 2048], P('ep'), may hold values from -0.1875 to 0.1875
- second_gain: bfloat16 [2048], replicated, may hold values from 0.099609375 to 1.8984375
- expert_ids: int32 [2048, 6], P(('grp', 'ep')), parts along dimension 0, may hold values from 0 to 63, all different within a row; in each aligned block of 8 rows (0 to 7, 8 to 15, ...) at most 2 rows name the same one
- route_weight: float32 [2048, 6], P(('grp', 'ep')), parts along dimension 0, may hold values from 0.2 to 1
- expert_gate: bfloat16 [64, 2048, 256], P('ep'), may hold values from -0.125 to 0.125
- expert_up: bfloat16 [64, 2048, 256], P('ep'), may hold values from -0.125 to 0.125
- expert_down: bfloat16 [64, 256, 2048], P('ep'), may hold values from -0.375 to 0.375
- shared_gate: bfloat16 [2048, 256], P('ep'), may hold values from -0.125 to 0.125
- shared_up: bfloat16 [2048, 256], P('ep'), may hold values from -0.125 to 0.125
- shared_down: bfloat16 [256, 2048], P(None, 'ep'), may hold values from -0.375 to 0.375
Outputs:
- mixed_out: bfloat16 [2048, 2048], P(('grp', 'ep')), parts along dimension 0
- memory_next: float32 [2048, 8, 128, 128], P(('grp', 'ep')), parts along dimension 0
- norm_next: float32 [2048, 8, 128], P(('grp', 'ep')), parts along dimension 0
- max_next: float32 [2048, 8], P(('grp', 'ep')), parts along dimension 0
There are 4 independent parts, one for each index of `grp`. A program takes and returns all parts, laid end to end along the dimension named above; an argument that names none is the same for every part. Nothing has to cross between parts.
Inputs may be any that keep to these rules, and one draw needn't show every extreme that they name: `expert_ids`: each row names 6 different experts. Among the rows of one device no expert is named by more than 2 rows, and in every draw some expert is named by exactly 2 rows of some device.
All inputs are finite; a program needn't handle non-finite values.
Results may differ from a plain program's by a relative error of at most 0.013.
Values may be sent and summed in bfloat16 or wider, within the bound.
No kernel may reach another device: no remote copies, remote signals or barrier semaphores. Data moves between devices by JAX's collectives and lax.ppermute only.
A program may use at most 64 MiB of HBM per device.

v0:
```python
import jax
import jax.numpy as jnp
from jax import lax
from jax.sharding import Mesh
from jax.sharding import PartitionSpec as P

FAR = "za"
NEAR = ("zm", "zb", "core")
ROW = ("za", "zm")
EP = ("za", "zm", "zb", "core")
GRP_EP = ("grp", "za", "zm", "zb", "core")
epsilon = 1e-06


def rms_scale(values, gain):
    return (
        values
        * lax.rsqrt(jnp.mean(values * values, axis=-1, keepdims=True) + epsilon)
        * gain.astype(jnp.float32)
    )


def cell_step(
    normed,
    query,
    key_proj,
    value_proj,
    outgate,
    igate_weight,
    fgate_weight,
    igate_bias,
    fgate_bias,
    memory_state,
    norm_state,
    max_state,
    head_gain,
):
    row_count, head_count = max_state.shape
    head_size = memory_state.shape[-1]
    input_gate = jnp.dot(normed, igate_weight, preferred_element_type=jnp.float32) + igate_bias
    forget_log = jax.nn.log_sigmoid(
        jnp.dot(normed, fgate_weight, preferred_element_type=jnp.float32) + fgate_bias
    )
    query_heads = query.astype(jnp.float32).reshape(row_count, head_count, head_size)
    key_heads = key_proj.astype(jnp.float32).reshape(
        row_count, head_count, head_size
    ) * head_size ** (-0.5)
    value_heads = value_proj.astype(jnp.float32).reshape(row_count, head_count, head_size)
    max_next = jnp.maximum(forget_log + max_state, input_gate)
    decay_rate = jnp.exp(forget_log + max_state - max_next)
    injected = jnp.exp(input_gate - max_next)
    memory_next = decay_rate[:, :, None, None] * memory_state + injected[:, :, None, None] * (
        key_heads[:, :, :, None] * value_heads[:, :, None, :]
    )
    norm_next = decay_rate[:, :, None] * norm_state + injected[:, :, None] * key_heads
    numerator = jnp.einsum(
        "shd,shde->she", query_heads, memory_next, precision=lax.Precision.HIGHEST
    )
    denominator = jnp.maximum(
        jnp.abs(jnp.sum(query_heads * norm_next, axis=-1)), jnp.exp(-max_next)
    )
    readout = numerator / denominator[:, :, None]
    readout = rms_scale(readout, head_gain.reshape(head_count, head_size))
    gated = readout.reshape(row_count, head_count * head_size) * jax.nn.sigmoid(
        outgate.astype(jnp.float32)
    )
    return (gated.astype(jnp.bfloat16), memory_next, norm_next, max_next)


def rounded(values, kind):
    info = jnp.finfo(kind)
    return lax.reduce_precision(values, info.nexp, info.nmant)


def from_peer(values, axis):
    return lax.ppermute(values, axis, [(0, 1), (1, 0)])


def in_order(values, axis_names, first):
    for place, name in enumerate(axis_names, first):
        values = jnp.where(lax.axis_index(name) == 0, values, jnp.flip(values, place))
    return values


def earlier_count(named, axis):
    count = named.shape[axis]
    before = jnp.arange(count)[:, None] < jnp.arange(count)[None, :]
    moved = jnp.moveaxis(named, axis, -1)
    counts = jnp.sum(jnp.where(before, moved[..., :, None], 0.0), axis=-2)
    return jnp.moveaxis(counts, -1, axis)


def split_two(values, kind):
    high = rounded(values, kind)
    return (high.astype(kind), (values - high).astype(kind))


def shards(
    tokens,
    first_gain,
    query_weight,
    key_weight,
    value_weight,
    outgate_weight,
    igate_weight,
    fgate_weight,
    igate_bias,
    fgate_bias,
    memory_state,
    norm_state,
    max_state,
    head_gain,
    out_weight,
    second_gain,
    expert_ids,
    route_weight,
    expert_gate,
    expert_up,
    expert_down,
    shared_gate,
    shared_up,
    shared_down,
):
    f32, bf16, f16 = (jnp.float32, jnp.bfloat16, jnp.float16)
    rows, width = tokens.shape
    top = expert_ids.shape[1]
    far = lax.axis_size(FAR)
    near = lax.axis_size(NEAR)
    row = lax.axis_size(ROW)
    devices = far * near
    members = devices // row
    slots = max(2, 2 * rows * top // devices)
    my_far = lax.axis_index(FAR)
    share = query_weight.shape[1]
    own = jnp.concatenate([query_weight.T, key_weight.T, value_weight.T, outgate_weight.T], axis=0)
    beside = from_peer(own, "zb")
    inputs = tokens.astype(f32)
    normed_exact = rounded(rms_scale(inputs, first_gain), bf16)
    normed = normed_exact.astype(bf16)
    weight_high, weight_low = split_two(route_weight, f16)
    notes = jnp.concatenate([expert_ids.astype(f16), weight_high, weight_low], axis=1)
    notes = jnp.pad(notes, ((0, 0), (0, 128 - notes.shape[1])))
    out_parts = out_weight.shape[0] // rows
    payload = jnp.concatenate(
        [normed_exact.astype(f16)]
        + [out_weight[i * rows : (i + 1) * rows].astype(f16) for i in range(out_parts)]
        + [notes],
        axis=1,
    )
    payload, beside = lax.optimization_barrier((payload, beside))
    column_weights = jnp.concatenate([own, beside], axis=0)
    other_weights = from_peer(column_weights, "core")
    gathered = lax.all_gather(payload, ROW, axis=0, tiled=True)
    block_rows = gathered[:, :width].astype(bf16)
    out_own = gathered[:, width : width * (1 + out_parts)]
    out_beside = from_peer(out_own, "zb")
    my_notes = gathered[:, width * (1 + out_parts) :].reshape(far, row // far, rows, 128)
    at_mine = lax.dynamic_index_in_dim(
        my_notes, lax.axis_index("zm"), axis=1, keepdims=False
    ).astype(f32)
    columns = jnp.concatenate(
        [
            lax.dot_general(
                block_rows, weights, (((1,), (1,)), ((), ())), preferred_element_type=f32
            )
            for weights in (column_weights, other_weights)
        ],
        axis=1,
    ).astype(bf16)
    projected = lax.all_to_all(
        columns.reshape(row, rows, columns.shape[1]), ROW, split_axis=0, concat_axis=0, tiled=True
    )
    projected, out_beside = lax.optimization_barrier((projected, out_beside))
    out_pair = jnp.stack([out_own, out_beside])
    out_other = from_peer(out_pair, "core")
    projected = projected.reshape(row, rows, 2, 2, 4, share).transpose(4, 1, 0, 3, 2, 5)
    projected = in_order(projected, ("zb", "core"), 3)
    projected = projected.reshape(4, rows, devices * share)
    slot_ids = jnp.arange(slots, dtype=f32)
    block_experts = (my_far * near).astype(f32) + jnp.arange(near, dtype=f32)
    hits = (at_mine[:, :, :top, None] == block_experts).astype(f32)
    weights = at_mine[:, :, top : 2 * top] + at_mine[:, :, 2 * top : 3 * top]
    hit = jnp.sum(hits, axis=2)
    hit_weight = jnp.sum(hits * weights[..., None], axis=2)
    hit_place = earlier_count(hit, 1)
    chosen = (hit_place[..., None] == slot_ids) * hit[..., None]
    same = (jnp.arange(far)[:, None] == jnp.arange(far))[:, None, None, :, None]
    chosen = jnp.where(same, chosen[:, :, :, None, :], 0.0)
    chosen = chosen.reshape(far * rows, near, far * slots)
    mixer = (chosen * hit_weight.reshape(far * rows, near, 1)).reshape(far * rows, -1)
    mixer_high, mixer_low = split_two(mixer, bf16)
    selector = chosen.reshape(far * rows, -1).astype(bf16)
    gated, memory_next, norm_next, max_next = cell_step(
        normed,
        projected[0],
        projected[1],
        projected[2],
        projected[3],
        igate_weight,
        fgate_weight,
        igate_bias,
        fgate_bias,
        memory_state,
        norm_state,
        max_state,
        head_gain,
    )
    spread = gated.reshape(rows, row, 2, 2, out_parts, -1).transpose(3, 2, 4, 0, 1, 5)
    spread = in_order(spread, ("core", "zb"), 0).reshape(2, 2, out_parts, rows, -1)
    mix_sums = jnp.zeros((rows, width), f32)
    for core, halves in enumerate((out_pair, out_other)):
        for zb in range(2):
            for part in range(out_parts):
                mix_sums = mix_sums + jnp.dot(
                    spread[core, zb, part],
                    halves[zb, :, part * width : (part + 1) * width].astype(bf16),
                    preferred_element_type=f32,
                )
    stream = inputs + mix_sums.astype(bf16).astype(f32)
    normed_exact = rounded(rms_scale(stream, second_gain), bf16)
    normed_two = normed_exact.astype(bf16)
    hidden = shared_gate.shape[1]
    depth = shared_gate.shape[0]
    cut = depth // rows
    piece = width // cut
    payload = jnp.concatenate(
        [
            jnp.concatenate(
                [normed_exact[:, i * piece : (i + 1) * piece] for i in range(cut)], axis=0
            ).astype(f16),
            shared_gate.astype(f16),
            shared_up.astype(f16),
            shared_down.T.astype(f16),
        ],
        axis=1,
    )
    gathered = lax.all_gather(payload, FAR, axis=0, tiled=True)
    far_rows = gathered[:, :piece].reshape(far, cut, rows, piece).transpose(0, 2, 1, 3)
    far_rows = far_rows.reshape(far * rows, width).astype(bf16)
    shared_one = gathered[:, piece:]
    shared_beside = from_peer(shared_one, "zm")
    outgoing = lax.dot_general(
        selector, far_rows, (((0,), (0,)), ((), ())), preferred_element_type=f32
    ).astype(bf16)
    flat_rows = lax.all_to_all(
        outgoing.reshape(near, far * slots, width), NEAR, split_axis=0, concat_axis=0, tiled=True
    ).reshape(near * far * slots, width)
    flat_rows, shared_beside = lax.optimization_barrier((flat_rows, shared_beside))
    shared_two = jnp.stack([shared_one, shared_beside])
    shared_beside = from_peer(shared_two, "zb")
    gate_sums = jnp.dot(flat_rows, expert_gate[0], preferred_element_type=f32)
    up_sums = jnp.dot(flat_rows, expert_up[0], preferred_element_type=f32)
    hidden_rows = (jax.nn.silu(gate_sums) * up_sums).astype(bf16)
    result = jnp.dot(hidden_rows, expert_down[0], preferred_element_type=f32).astype(bf16)
    near_results = lax.all_to_all(
        result.reshape(near, far * slots, width), NEAR, split_axis=0, concat_axis=0, tiled=True
    ).reshape(near * far * slots, width)
    near_results, shared_beside = lax.optimization_barrier((near_results, shared_beside))
    shared_four = jnp.stack([shared_two, shared_beside])
    shared_other = from_peer(shared_four, "core")
    partial = jnp.dot(mixer_high, near_results, preferred_element_type=f32) + jnp.dot(
        mixer_low, near_results, preferred_element_type=f32
    )
    far_sums = lax.all_to_all(
        partial.astype(bf16).reshape(far, rows, width), FAR, split_axis=0, concat_axis=0, tiled=True
    )
    routed = jnp.sum(far_sums.astype(f32), axis=0)
    by_member = normed_two.reshape(rows, far, 2, 2, 2, depth).transpose(4, 3, 2, 0, 1, 5)
    by_member = in_order(by_member, ("core", "zb", "zm"), 0).reshape(near, rows, far * depth)
    shared_all = jnp.concatenate(
        [
            shared_four.reshape(near // 2, far * depth, -1),
            shared_other.reshape(near // 2, far * depth, -1),
        ]
    ).astype(bf16)
    gate_up = lax.dot_general(
        by_member,
        shared_all[:, :, : 2 * hidden],
        (((2,), (1,)), ((0,), (0,))),
        preferred_element_type=f32,
    )
    gate_up = jnp.sum(gate_up, axis=0)
    hidden_shared = (jax.nn.silu(gate_up[:, :hidden]) * gate_up[:, hidden:]).astype(bf16)
    shared_result = lax.dot_general(
        hidden_shared,
        shared_all[:, :, 2 * hidden :],
        (((1,), (2,)), ((), ())),
        preferred_element_type=f32,
    )
    shared_result = shared_result.reshape(rows, 2, 2, 2, far, depth).transpose(0, 4, 3, 2, 1, 5)
    shared_result = in_order(shared_result, NEAR, 2).reshape(rows, width)
    mixed_out = (stream + routed + shared_result).astype(bf16)
    return (mixed_out, memory_next, norm_next, max_next)


def solution(mesh):
    torus = Mesh(mesh.devices.reshape(mesh.shape["grp"], 8, 2, 2, 2), GRP_EP)
    placed = (
        P(GRP_EP, None),
        P(),
        P(None, EP),
        P(None, EP),
        P(None, EP),
        P(None, EP),
        P(),
        P(),
        P(),
        P(),
        P(GRP_EP, None, None, None),
        P(GRP_EP, None, None),
        P(GRP_EP, None),
        P(),
        P(EP, None),
        P(),
        P(GRP_EP, None),
        P(GRP_EP, None),
        P(EP, None, None),
        P(EP, None, None),
        P(EP, None, None),
        P(EP, None),
        P(EP, None),
        P(None, EP),
    )
    return jax.shard_map(
        shards,
        mesh=torus,
        in_specs=placed,
        out_specs=(
            P(GRP_EP, None),
            P(GRP_EP, None, None, None),
            P(GRP_EP, None, None),
            P(GRP_EP, None),
        ),
        check_vma=False,
    )
```

profile of v0, /device:TPU:102, one launch (start us, length us, event | category | flops | bytes accessed | tf_op | source)
XLA Modules:
  0.0 358.0 jit_solution(3707160827783618954)
XLA Ops:
  1.9 1.5 constant_dynamic-update-slice_fusion.4
  9.4 1.6 broadcast_multiply_fusion.1
  13.0 1.5 constant_dynamic-update-slice_fusion.3
  14.5 1.5 constant_dynamic-update-slice_fusion.2
  15.9 1.5 constant_dynamic-update-slice_fusion.1
  22.8 79.3 %all-gather.1 = f16[128,6272]{1,0:T(8,128)(2,1)S(1)} all-gather(f16[8,6272]{1,0:T(8,128)(2,1)S(1)} %pad_maximum_fusion.4), channel_id=1, replica_groups=mesh['grp'=4,'za'=8,'zm'=2,'zb'=2,'core'=2] {'za','zm'}, dimensions={0}, use_global_device_ids=true | all-gather | bytes 1705984 | tf_op jit(solution)/shard_map/all_gather | solution.py:153
  106.5 1.5 fusion.10
  108.0 1.5 fusion.11
  110.2 8.9 %all-to-all-start = ((bf16[16,8,256]{2,1,0:T(8,128)(2,1)}), bf16[16,8,256]{2,1,0:T(8,128)(2,1)S(1)}, u32[]{:S(2)}, u32[]{:S(2)}) async-start(bf16[16,8,256]{2,1,0:T(8,128)(2,1)} %pad_maximum_fusion.6), calls=%async_computation | async-start | bytes 131072 | tf_op jit(solution)/shard_map/all_to_all | solution.py:170
  120.2 23.3 %all-to-all-done = bf16[16,8,256]{2,1,0:T(8,128)(2,1)S(1)} async-done(((bf16[16,8,256]{2,1,0:T(8,128)(2,1)}), bf16[16,8,256]{2,1,0:T(8,128)(2,1)S(1)}, u32[]{:S(2)}, u32[]{:S(2)}) %all-to-all-start) | async-done | bytes 65568 | tf_op jit(solution)/shard_map/all_to_all | solution.py:170
  149.5 1.8 copy.62
  151.3 1.9 reshape.215
  153.2 1.5 multiply_reduce_fusion.2
  155.4 1.8 copy.63
  157.1 1.9 reshape.216
  160.1 1.8 pad_maximum_fusion
  163.0 2.6 multiply_add_fusion
  165.6 2.0 fusion.82
  167.9 1.6 reshape.201
  169.5 1.5 fusion.46
  177.9 45.1 %all_gather.7 = f16[256,1280]{1,0:T(8,128)(2,1)S(1)} all-gather(f16[32,1280]{1,0:T(8,128)(2,1)S(1)} %pad_maximum_fusion.5), channel_id=1, replica_groups=mesh['grp'=4,'za'=8,'zm'=2,'zb'=2,'core'=2] {'za'}, dimensions={0}, use_global_device_ids=true | all-gather | bytes 737280 | tf_op jit(solution)/shard_map/all_gather | solution.py:237
  224.1 3.6 all-to-all-start.1
  227.8 2.2 collective-permute-start.4
  230.0 26.1 %collective-permute-done.4 = f16[256,768]{1,0:T(8,128)(2,1)S(1)} collective-permute-done((f16[256,768]{1,0:T(8,128)(2,1)S(1)}, f16[256,768]{1,0:T(8,128)(2,1)S(1)}, u32[]{:S(2)}, u32[]{:S(2)}) %collective-permute-start.4) | collective-permute-done | bytes 393248 | tf_op jit(solution)/shard_map/ppermute | solution.py:76
  256.1 1.5 fusion.22
  257.6 2.8 convolution_convert_fusion
  260.5 7.0 %all-to-all-start.2 = ((bf16[8,16,2048]{2,1,0:T(8,128)(2,1)}), bf16[8,16,2048]{2,1,0:T(8,128)(2,1)S(1)}, u32[]{:S(2)}, u32[]{:S(2)}) async-start(bf16[8,16,2048]{2,1,0:T(8,128)(2,1)} %bitcast.47), calls=%async_computation.2 | async-start | bytes 1048576 | tf_op jit(solution)/shard_map/all_to_all | solution.py:255
  268.8 25.5 %collective-permute-done.5 = f16[2,256,768]{2,1,0:T(8,128)(2,1)S(1)} collective-permute-done((f16[2,256,768]{2,1,0:T(8,128)(2,1)S(1)}, f16[2,256,768]{2,1,0:T(8,128)(2,1)S(1)}, u32[]{:S(2)}, u32[]{:S(2)}) %collective-permute-start.5) | collective-permute-done | bytes 786464 | tf_op jit(solution)/shard_map/ppermute | solution.py:76
  295.2 1.7 pad_maximum_fusion.1
  301.6 14.4 %all-to-all-start.3 = ((bf16[8,8,2048]{2,1,0:T(8,128)(2,1)}), bf16[8,8,2048]{2,1,0:T(8,128)(2,1)S(1)}, u32[]{:S(2)}, u32[]{:S(2)}) async-start(bf16[8,8,2048]{2,1,0:T(8,128)(2,1)} %fusion.1), calls=%async_computation.3 | async-start | bytes 524288 | tf_op jit(solution)/shard_map/all_to_all | solution.py:264
  316.6 1.9 maximum_convert_fusion
  322.2 35.1 %all-to-all-done.3 = bf16[8,8,2048]{2,1,0:T(8,128)(2,1)S(1)} async-done(((bf16[8,8,2048]{2,1,0:T(8,128)(2,1)}), bf16[8,8,2048]{2,1,0:T(8,128)(2,1)S(1)}, u32[]{:S(2)}, u32[]{:S(2)}) %all-to-all-start.3) | async-done | bytes 262176 | tf_op jit(solution)/shard_map/all_to_all | solution.py:264
  (146 shorter events, 49.6 us)
Async XLA Ops:
  0.6 257.0 %copy-start = (bf16[1,256,2048]{2,1,0:T(8,128)(2,1)S(1)}, bf16[1,256,2048]{2,1,0:T(8,128)(2,1)}, u32[]{:S(2)}) copy-start(bf16[1,256,2048]{2,1,0:T(8,128)(2,1)} %param.44) | copy-start | bytes 3145732
  1.7 21.1 %collective-permute-start = (bf16[64,2048]{1,0:T(8,128)(2,1)S(1)}, bf16[64,2048]{1,0:T(8,128)(2,1)S(1)}, u32[]{:S(2)}, u32[]{:S(2)}) collective-permute-start(bf16[64,2048]{1,0:T(8,128)(2,1)S(1)} %pad_maximum_fusion.3), channel_id=1, source_target_pairs={{0,2},{2,0},{1,3},{3,1},{4,6},{6,4},{5,7},{7,5},{8,10},{10,8},{9,1... | collective-permute-start | bytes 786440 | tf_op jit(solution)/shard_map/ppermute | solution.py:76
  1.9 117.5 %copy-start.16 = (pred[8,8]{0,1:T(8,128)(4,1)}, pred[8,8]{0,1:T(8,128)(4,1)S(1)}, u32[]{:S(2)}) copy-start(pred[8,8]{0,1:T(8,128)(4,1)S(1)} %iota_compare_fusion.3) | copy-start | bytes 196
  11.0 0.6 copy-start.13
  102.0 1.2 copy-start.2
  105.2 2.8 collective-permute-start.1
  105.5 38.1 %collective-permute-start.2 = (f16[128,4096]{1,0:T(8,128)(2,1)}, f16[128,4096]{1,0:T(8,128)(2,1)S(1)}, u32[]{:S(2)}, u32[]{:S(2)}) collective-permute-start(f16[128,4096]{1,0:T(8,128)(2,1)} %get-tuple-element.28), channel_id=1, source_target_pairs={{0,2},{2,0},{1,3},{3,1},{4,6},{6,4},{5,7},{7,5},{8,10},{10,8},{9,1... | collective-permute-start | bytes 3145736 | tf_op jit(solution)/shard_map/ppermute | solution.py:76
  110.2 33.4 %all-to-all-start = ((bf16[16,8,256]{2,1,0:T(8,128)(2,1)}), bf16[16,8,256]{2,1,0:T(8,128)(2,1)S(1)}, u32[]{:S(2)}, u32[]{:S(2)}) async-start(bf16[16,8,256]{2,1,0:T(8,128)(2,1)} %pad_maximum_fusion.6), calls=%async_computation | async-start | bytes 131072 | tf_op jit(solution)/shard_map/all_to_all | solution.py:170
  159.0 2.9 copy-start.11
  159.0 2.9 copy-start.15
  160.1 2.9 copy-start.3
  161.9 10.8 %collective-permute-start.3 = (f16[2,128,4096]{2,1,0:T(8,128)(2,1)}, f16[2,128,4096]{2,1,0:T(8,128)(2,1)}, u32[]{:S(2)}, u32[]{:S(2)}) collective-permute-start(f16[2,128,4096]{2,1,0:T(8,128)(2,1)} %pad_maximum_fusion), channel_id=1, source_target_pairs={{0,1},{1,0},{2,3},{3,2},{4,5},{5,4},{6,7},{7,6},{8,9},{9,8},{10,11... | collective-permute-start | bytes 6291464 | tf_op jit(solution)/shard_map/ppermute | solution.py:76
  165.6 2.0 copy-start.1
  165.6 2.2 copy-start.14
  171.9 4.5 %copy-start.5 = (bf16[8,2048]{1,0:T(8,128)(2,1)S(1)}, bf16[8,2048]{1,0:T(8,128)(2,1)}, u32[]{:S(2)}) copy-start(bf16[8,2048]{1,0:T(8,128)(2,1)} %param.24) | copy-start | bytes 98308
  172.2 5.4 %copy-start.12 = (f32[2048]{0:T(1024)S(1)}, f32[2048]{0:T(1024)}, u32[]{:S(2)}) copy-start(f32[2048]{0:T(1024)} %convert_element_type.262) | copy-start | bytes 24580
  172.2 5.6 %copy-start.8 = (f16[32,256]{1,0:T(8,128)(2,1)S(1)}, f16[32,256]{1,0:T(8,128)(2,1)}, u32[]{:S(2)}) copy-start(f16[32,256]{1,0:T(8,128)(2,1)} %convert_element_type.263) | copy-start | bytes 49156
  172.2 5.6 %copy-start.9 = (f16[32,256]{1,0:T(8,128)(2,1)S(1)}, f16[32,256]{1,0:T(8,128)(2,1)}, u32[]{:S(2)}) copy-start(f16[32,256]{1,0:T(8,128)(2,1)} %convert_element_type.264) | copy-start | bytes 49156
  172.3 5.6 %copy-start.10 = (f16[32,256]{1,0:T(8,128)(2,1)S(1)}, f16[32,256]{1,0:T(8,128)(2,1)}, u32[]{:S(2)}) copy-start(f16[32,256]{1,0:T(8,128)(2,1)} %convert_bitcast_fusion) | copy-start | bytes 49156
  172.6 50.4 %copy-start.6 = (bf16[64,128]{0,1:T(8,128)(2,1)S(1)}, bf16[64,128]{0,1:T(8,128)(2,1)}, u32[]{:S(2)}) copy-start(bf16[64,128]{0,1:T(8,128)(2,1)} %convert_element_type.261) | copy-start | bytes 49156
  224.1 32.0 %all-to-all-start.1 = ((bf16[8,16,2048]{2,1,0:T(8,128)(2,1)}), bf16[8,16,2048]{2,1,0:T(8,128)(2,1)S(1)}, u32[]{:S(2)}, u32[]{:S(2)}) async-start(bf16[8,16,2048]{2,1,0:T(8,128)(2,1)} %bitcast.42), calls=%async_computation.1 | async-start | bytes 1048576 | tf_op jit(solution)/shard_map/all_to_all | solution.py:245
  227.8 28.3 %collective-permute-start.4 = (f16[256,768]{1,0:T(8,128)(2,1)S(1)}, f16[256,768]{1,0:T(8,128)(2,1)S(1)}, u32[]{:S(2)}, u32[]{:S(2)}) collective-permute-start(f16[256,768]{1,0:T(8,128)(2,1)S(1)} %get-tuple-element.32), channel_id=1, source_target_pairs={{0,4},{4,0},{1,5},{5,1},{2,6},{6,2},{3,7},{7,3},{8,12},{12,8},{9,1... | collective-permute-start | bytes 1179656 | tf_op jit(solution)/shard_map/ppermute | solution.py:76
  260.5 33.8 %all-to-all-start.2 = ((bf16[8,16,2048]{2,1,0:T(8,128)(2,1)}), bf16[8,16,2048]{2,1,0:T(8,128)(2,1)S(1)}, u32[]{:S(2)}, u32[]{:S(2)}) async-start(bf16[8,16,2048]{2,1,0:T(8,128)(2,1)} %bitcast.47), calls=%async_computation.2 | async-start | bytes 1048576 | tf_op jit(solution)/shard_map/all_to_all | solution.py:255
  268.5 28.6 %copy-start.17 = (pred[8,8]{0,1:T(8,128)(4,1)S(1)}, pred[8,8]{0,1:T(8,128)(4,1)}, u32[]{:S(2)}) copy-start(pred[8,8]{0,1:T(8,128)(4,1)} %copy-done.16) | copy-start | bytes 196
  268.5 28.8 %copy-start.7 = (f32[8,8,8]{2,1,0:T(8,128)S(1)}, f32[8,8,8]{2,1,0:T(8,128)}, u32[]{:S(2)}) copy-start(f32[8,8,8]{2,1,0:T(8,128)} %get-tuple-element.20) | copy-start | bytes 6148
  268.5 25.8 %collective-permute-start.5 = (f16[2,256,768]{2,1,0:T(8,128)(2,1)S(1)}, f16[2,256,768]{2,1,0:T(8,128)(2,1)S(1)}, u32[]{:S(2)}, u32[]{:S(2)}) collective-permute-start(f16[2,256,768]{2,1,0:T(8,128)(2,1)S(1)} %get-tuple-element.30), channel_id=1, source_target_pairs={{0,2},{2,0},{1,3},{3,1},{4,6},{6,4},{5,7},{7,5},{8,10},{10,8},{9,1... | collective-permute-start | bytes 2359304 | tf_op jit(solution)/shard_map/ppermute | solution.py:76
  294.3 0.9 copy-start.4
  297.0 19.7 %collective-permute-start.6 = (f16[2,2,256,768]{3,2,1,0:T(8,128)(2,1)S(1)}, f16[2,2,256,768]{3,2,1,0:T(8,128)(2,1)}, u32[]{:S(2)}, u32[]{:S(2)}) collective-permute-start(f16[2,2,256,768]{3,2,1,0:T(8,128)(2,1)S(1)} %pad_maximum_fusion.1), channel_id=1, source_target_pairs={{0,1},{1,0},{2,3},{3,2},{4,5},{5,4},{6,7},{7,6},{8,9},{9,8},{10,11... | collective-permute-start | bytes 4718600 | tf_op jit(solution)/shard_map/ppermute | solution.py:76
  301.6 55.7 %all-to-all-start.3 = ((bf16[8,8,2048]{2,1,0:T(8,128)(2,1)}), bf16[8,8,2048]{2,1,0:T(8,128)(2,1)S(1)}, u32[]{:S(2)}, u32[]{:S(2)}) async-start(bf16[8,8,2048]{2,1,0:T(8,128)(2,1)} %fusion.1), calls=%async_computation.3 | async-start | bytes 524288 | tf_op jit(solution)/shard_map/all_to_all | solution.py:264
where the time goes:
time: 360 us; the launch traced here: 358 us
  blocking collectives  124 us (34%)
  waiting for transfers between devices  110 us (31%)
  starting transfers between devices  36.7 us (10%)
  local copies, waits for them, and re-layouts  31.9 us (9%)
  other arithmetic  31.9 us (9%)
  matrix products  21.8 us (6%)
    all_gather x1, blocking collectives, shards(): gathered = lax.all_gather(payload, ROW, axis=0, tiled=True)  79.3 us
    ppermute x7, waiting for transfers between devices, from_peer(): return lax.ppermute(values, axis, [(0, 1), (1, 0)])  51.6 us
    all_gather x1, blocking collectives, shards(): gathered = lax.all_gather(payload, FAR, axis=0, tiled=True)  45.1 us
    all_to_all x1, waiting for transfers between devices, shards(): lax.all_to_all(partial.astype(bf16).reshape(far, rows, width), FAR, split...  35.1 us
    all_to_all x1, waiting for transfers between devices, shards(): lax.all_to_all(columns.reshape(row, rows, columns.shape[1]), ROW, split_a...  23.3 us
    all_to_all x1, starting transfers between devices, shards(): lax.all_to_all(partial.astype(bf16).reshape(far, rows, width), FAR, split...  14.4 us
    unnamed x40, local copies, waits for them, and re-layouts  9.69 us
    all_to_all x1, starting transfers between devices, shards(): lax.all_to_all(columns.reshape(row, rows, columns.shape[1]), ROW, split_a...  8.88 us
  transfers between devices with their start and end apart: 11, of which 4 were waited for; matrix products, arithmetic and copies ran while one was open for 13% of the time, Pallas kernels for 0%

commit v1 on v0

--- a/solution.py
+++ b/solution.py
@@ -1,3 +1,4 @@
+import functools
 import jax
 import jax.numpy as jnp
 from jax import lax
@@ -10,6 +11,16 @@
 EP = ("za", "zm", "zb", "core")
 GRP_EP = ("grp", "za", "zm", "zb", "core")
 epsilon = 1e-06
+
+
+def keep_up_stops_all(point, mesh_ax):
+    leaves = []
+    for _ in range(lax.axis_size(mesh_ax)):
+        leaves.append(point)
+    return jnp.concatenate(lax.all_to_all(jnp.stack(leaves, 0), mesh_ax, 0, 0), 0)
+
+
+supply_marks_here = functools.partial(keep_up_stops_all, mesh_ax=FAR)
 
 
 def rms_scale(values, gain):
@@ -234,7 +245,7 @@
         ],
         axis=1,
     )
-    gathered = lax.all_gather(payload, FAR, axis=0, tiled=True)
+    gathered = supply_marks_here(payload)
     far_rows = gathered[:, :piece].reshape(far, cut, rows, piece).transpose(0, 2, 1, 3)
     far_rows = far_rows.reshape(far * rows, width).astype(bf16)
     shared_one = gathered[:, piece:]

time: 360 us -> 373 us (1.036)
  waiting for transfers between devices: 110 us -> 175 us
  blocking collectives: 124 us -> 74.4 us
  starting transfers between devices: 36.7 us -> 48.6 us
  other arithmetic: 31.9 us -> 25.6 us
  local copies, waits for them, and re-layouts: 31.9 us -> 26.3 us
    all_to_all x0 -> x1, waiting for transfers between devices: none -> 69.2 us  [keep_up_stops_all(): lax.all_to_all(jnp.stack(leaves, 0), mesh_ax, 0, 0)]
    all_gather x1 -> x0, blocking collectives: 45.1 us -> none  [shards(): gathered = lax.all_gather(payload, FAR, axis=0, tiled=True)]
    all_to_all x1, starting transfers between devices: 14.4 us -> 3.84 us  [shards(): lax.all_to_all(partial.astype(bf16).reshape(far, rows, width), FAR, split...]
    all_to_all x1, starting transfers between devices: 8.88 us -> 17 us  [shards(): lax.all_to_all(columns.reshape(row, rows, columns.shape[1]), ROW, split_a...]
    all_to_all x1, starting transfers between devices: 3.57 us -> 8.97 us  [shards(): lax.all_to_all(outgoing.reshape(near, far * slots, width), NEAR, split_ax...]
    ppermute x7, starting transfers between devices: 2.91 us -> 7.86 us  [from_peer(): return lax.ppermute(values, axis, [(0, 1), (1, 0)])]
    all_gather x1, blocking collectives: 79.3 us -> 74.4 us  [shards(): gathered = lax.all_gather(payload, ROW, axis=0, tiled=True)]
    unnamed x40 -> x38, local copies, waits for them, and re-layouts: 9.69 us -> 5.52 us
  transfers between devices with their start and end apart: 11 -> 12, of which waited for: 4 -> 5; matrix products, arithmetic and copies ran while one was open for 13% -> 10% of each run, Pallas kernels for 0% -> 0%
where the time goes in v1:
time: 373 us; the launch traced here: 371 us
  waiting for transfers between devices  175 us (47%)
  blocking collectives  74.4 us (20%)
  starting transfers between devices  48.6 us (13%)
  local copies, waits for them, and re-layouts  26.3 us (7%)
  other arithmetic  25.6 us (7%)
  matrix products  19.4 us (5%)
    all_gather x1, blocking collectives, shards(): gathered = lax.all_gather(payload, ROW, axis=0, tiled=True)  74.4 us
    all_to_all x1, waiting for transfers between devices, keep_up_stops_all(): lax.all_to_all(jnp.stack(leaves, 0), mesh_ax, 0, 0)  69.2 us
    ppermute x7, waiting for transfers between devices, from_peer(): return lax.ppermute(values, axis, [(0, 1), (1, 0)])  51.6 us
    all_to_all x1, waiting for transfers between devices, shards(): lax.all_to_all(partial.astype(bf16).reshape(far, rows, width), FAR, split...  35 us
    all_to_all x1, waiting for transfers between devices, shards(): lax.all_to_all(columns.reshape(row, rows, columns.shape[1]), ROW, split_a...  19.4 us
    all_to_all x1, starting transfers between devices, shards(): lax.all_to_all(columns.reshape(row, rows, columns.shape[1]), ROW, split_a...  17 us
    all_to_all x1, starting transfers between devices, shards(): lax.all_to_all(outgoing.reshape(near, far * slots, width), NEAR, split_ax...  8.97 us
    ppermute x7, starting transfers between devices, from_peer(): return lax.ppermute(values, axis, [(0, 1), (1, 0)])  7.86 us
  transfers between devices with their start and end apart: 12, of which 5 were waited for; matrix products, arithmetic and copies ran while one was open for 10% of the time, Pallas kernels for 0%

profile of v1, /device:TPU:102, one launch (start us, length us, event | category | flops | bytes accessed | tf_op | source)
XLA Modules:
  0.0 370.7 jit_solution(16074158664609318631)
XLA Ops:
  10.9 1.6 broadcast_multiply_fusion.1
  12.7 74.4 %all-gather.1 = f16[128,6272]{1,0:T(8,128)(2,1)S(1)} all-gather(f16[8,6272]{1,0:T(8,128)(2,1)S(1)} %pad_maximum_fusion.4), channel_id=1, replica_groups=mesh['grp'=4,'za'=8,'zm'=2,'zb'=2,'core'=2] {'za','zm'}, dimensions={0}, use_global_device_ids=true | all-gather | bytes 1705984 | tf_op jit(solution)/shard_map/all_gather | solution.py:164
  87.1 1.5 slice_bitcast_fusion.17
  88.6 4.7 %collective-permute-start.2 = (f16[128,4096]{1,0:T(8,128)(2,1)}, f16[128,4096]{1,0:T(8,128)(2,1)S(1)}, u32[]{:S(2)}, u32[]{:S(2)}) collective-permute-start(f16[128,4096]{1,0:T(8,128)(2,1)} %get-tuple-element.28), channel_id=1, source_target_pairs={{0,2},{2,0},{1,3},{3,1},{4,6},{6,4},{5,7},{7,5},{8,10},{10,8},{9,1... | collective-permute-start | bytes 3145736 | tf_op jit(solution)/shard_map/ppermute | solution.py:87
  94.5 17.0 %all-to-all-start = ((bf16[16,8,256]{2,1,0:T(8,128)(2,1)}), bf16[16,8,256]{2,1,0:T(8,128)(2,1)S(1)}, u32[]{:S(2)}, u32[]{:S(2)}) async-start(bf16[16,8,256]{2,1,0:T(8,128)(2,1)} %pad_maximum_fusion.6), calls=%async_computation | async-start | bytes 131072 | tf_op jit(solution)/shard_map/all_to_all | solution.py:181
  114.0 19.4 %all-to-all-done = bf16[16,8,256]{2,1,0:T(8,128)(2,1)S(1)} async-done(((bf16[16,8,256]{2,1,0:T(8,128)(2,1)}), bf16[16,8,256]{2,1,0:T(8,128)(2,1)S(1)}, u32[]{:S(2)}, u32[]{:S(2)}) %all-to-all-start) | async-done | bytes 65568 | tf_op jit(solution)/shard_map/all_to_all | solution.py:181
  134.6 1.4 copy.79
  139.4 1.8 copy.62
  141.2 1.3 reshape.221
  142.4 1.5 multiply_reduce_fusion.2
  144.6 1.8 copy.63
  146.4 1.3 reshape.222
  148.7 1.8 pad_maximum_fusion
  151.6 1.6 multiply_add_fusion
  153.2 2.0 fusion.82
  155.5 1.6 reshape.206
  157.1 1.5 fusion.46
  163.9 1.3 multiply_reduce_fusion
  166.4 4.0 %all-to-all-start.1 = ((f16[8,32,1280]{2,1,0:T(8,128)(2,1)}), f16[8,32,1280]{2,1,0:T(8,128)(2,1)S(1)}, u32[]{:S(2)}, u32[]{:S(2)}) async-start(f16[8,32,1280]{2,1,0:T(8,128)(2,1)} %stack.41), calls=%async_computation.1 | async-start | bytes 1310720 | tf_op jit(solution)/shard_map/all_to_all | solution.py:20
  171.6 69.2 %all-to-all-done.1 = f16[8,32,1280]{2,1,0:T(8,128)(2,1)S(1)} async-done(((f16[8,32,1280]{2,1,0:T(8,128)(2,1)}), f16[8,32,1280]{2,1,0:T(8,128)(2,1)S(1)}, u32[]{:S(2)}, u32[]{:S(2)}) %all-to-all-start.1) | async-done | bytes 655392 | tf_op jit(solution)/shard_map/all_to_all | solution.py:20
  241.8 9.0 %all-to-all-start.2 = ((bf16[8,16,2048]{2,1,0:T(8,128)(2,1)}), bf16[8,16,2048]{2,1,0:T(8,128)(2,1)S(1)}, u32[]{:S(2)}, u32[]{:S(2)}) async-start(bf16[8,16,2048]{2,1,0:T(8,128)(2,1)} %bitcast.43), calls=%async_computation.2 | async-start | bytes 1048576 | tf_op jit(solution)/shard_map/all_to_all | solution.py:256
  250.9 2.5 collective-permute-start.4
  253.4 26.1 %collective-permute-done.4 = f16[256,768]{1,0:T(8,128)(2,1)S(1)} collective-permute-done((f16[256,768]{1,0:T(8,128)(2,1)S(1)}, f16[256,768]{1,0:T(8,128)(2,1)S(1)}, u32[]{:S(2)}, u32[]{:S(2)}) %collective-permute-start.4) | collective-permute-done | bytes 393248 | tf_op jit(solution)/shard_map/ppermute | solution.py:87
  279.5 1.5 fusion.22
  281.0 2.8 convolution_convert_fusion
  283.8 6.9 %all-to-all-start.3 = ((bf16[8,16,2048]{2,1,0:T(8,128)(2,1)}), bf16[8,16,2048]{2,1,0:T(8,128)(2,1)S(1)}, u32[]{:S(2)}, u32[]{:S(2)}) async-start(bf16[8,16,2048]{2,1,0:T(8,128)(2,1)} %bitcast.48), calls=%async_computation.3 | async-start | bytes 1048576 | tf_op jit(solution)/shard_map/all_to_all | solution.py:266
  292.1 25.5 %collective-permute-done.5 = f16[2,256,768]{2,1,0:T(8,128)(2,1)S(1)} collective-permute-done((f16[2,256,768]{2,1,0:T(8,128)(2,1)S(1)}, f16[2,256,768]{2,1,0:T(8,128)(2,1)S(1)}, u32[]{:S(2)}, u32[]{:S(2)}) %collective-permute-start.5) | collective-permute-done | bytes 786464 | tf_op jit(solution)/shard_map/ppermute | solution.py:87
  318.6 1.7 pad_maximum_fusion.1
  324.9 3.8 %all-to-all-start.4 = ((bf16[8,8,2048]{2,1,0:T(8,128)(2,1)}), bf16[8,8,2048]{2,1,0:T(8,128)(2,1)S(1)}, u32[]{:S(2)}, u32[]{:S(2)}) async-start(bf16[8,8,2048]{2,1,0:T(8,128)(2,1)} %fusion.1), calls=%async_computation.4 | async-start | bytes 524288 | tf_op jit(solution)/shard_map/all_to_all | solution.py:275
  329.4 1.9 maximum_convert_fusion
  331.8 1.4 fusion.16
  335.0 35.0 %all-to-all-done.4 = bf16[8,8,2048]{2,1,0:T(8,128)(2,1)S(1)} async-done(((bf16[8,8,2048]{2,1,0:T(8,128)(2,1)}), bf16[8,8,2048]{2,1,0:T(8,128)(2,1)S(1)}, u32[]{:S(2)}, u32[]{:S(2)}) %all-to-all-start.4) | async-done | bytes 262176 | tf_op jit(solution)/shard_map/all_to_all | solution.py:275
  (147 shorter events, 40.8 us)
Async XLA Ops:
  0.6 280.4 %copy-start = (bf16[1,256,2048]{2,1,0:T(8,128)(2,1)S(1)}, bf16[1,256,2048]{2,1,0:T(8,128)(2,1)}, u32[]{:S(2)}) copy-start(bf16[1,256,2048]{2,1,0:T(8,128)(2,1)} %param.44) | copy-start | bytes 3145732
  1.7 10.9 %collective-permute-start = (bf16[64,2048]{1,0:T(8,128)(2,1)S(1)}, bf16[64,2048]{1,0:T(8,128)(2,1)S(1)}, u32[]{:S(2)}, u32[]{:S(2)}) collective-permute-start(bf16[64,2048]{1,0:T(8,128)(2,1)S(1)} %pad_maximum_fusion.3), channel_id=1, source_target_pairs={{0,2},{2,0},{1,3},{3,1},{4,6},{6,4},{5,7},{7,5},{8,10},{10,8},{9,1... | collective-permute-start | bytes 786440 | tf_op jit(solution)/shard_map/ppermute | solution.py:87
  12.5 100.3 %copy-start.9 = (f32[8,8]{1,0:T(8,128)}, f32[8,8]{1,0:T(8,128)S(1)}, u32[]{:S(2)}) copy-start(f32[8,8]{1,0:T(8,128)S(1)} %get-tuple-element.26) | copy-start | bytes 772
  12.6 81.0 %collective-permute-start.1 = (bf16[128,2048]{1,0:T(8,128)(2,1)S(1)}, bf16[128,2048]{1,0:T(8,128)(2,1)S(1)}, u32[]{:S(2)}, u32[]{:S(2)}) collective-permute-start(bf16[128,2048]{1,0:T(8,128)(2,1)S(1)} %constant_dynamic-update-slice_fusion), channel_id=1, source_target_pairs={{0,1},{1,0},{2,3},{3,2},{4,5},{5,4},{6,7},{7,6},{8,9},{9,8},{10,11... | collective-permute-start | bytes 1572872 | tf_op jit(solution)/shard_map/ppermute | solution.py:87
  87.1 6.5 %copy-start.2 = (f16[128,6272]{1,0:T(8,128)(2,1)}, f16[128,6272]{1,0:T(8,128)(2,1)S(1)}, u32[]{:S(2)}) copy-start(f16[128,6272]{1,0:T(8,128)(2,1)S(1)} %all-gather.1) | copy-start | bytes 4816900
  87.1 24.5 %copy-start.16 = (bf16[1024]{0:T(1024)(128)(2,1)S(1)}, bf16[1024]{0:T(1024)(128)(2,1)}, u32[]{:S(2)}) copy-start(bf16[1024]{0:T(1024)(128)(2,1)} %param.37) | copy-start | bytes 6148
  87.1 25.1 %copy-start.15 = (bf16[2048]{0:T(1024)(128)(2,1)S(1)}, bf16[2048]{0:T(1024)(128)(2,1)}, u32[]{:S(2)}) copy-start(bf16[2048]{0:T(1024)(128)(2,1)} %param.39) | copy-start | bytes 12292
  87.1 25.7 %copy-start.11 = (bf16[32,256]{1,0:T(8,128)(2,1)S(1)}, bf16[32,256]{1,0:T(8,128)(2,1)}, u32[]{:S(2)}) copy-start(bf16[32,256]{1,0:T(8,128)(2,1)} %param.45) | copy-start | bytes 49156
  87.1 25.7 %copy-start.12 = (bf16[32,256]{1,0:T(8,128)(2,1)S(1)}, bf16[32,256]{1,0:T(8,128)(2,1)}, u32[]{:S(2)}) copy-start(bf16[32,256]{1,0:T(8,128)(2,1)} %param.46) | copy-start | bytes 49156
  87.1 26.3 %copy-start.13 = (bf16[256,32]{0,1:T(8,128)(2,1)S(1)}, bf16[256,32]{0,1:T(8,128)(2,1)}, u32[]{:S(2)}) copy-start(bf16[256,32]{0,1:T(8,128)(2,1)} %param.47) | copy-start | bytes 49156
  88.6 44.8 %collective-permute-start.2 = (f16[128,4096]{1,0:T(8,128)(2,1)}, f16[128,4096]{1,0:T(8,128)(2,1)S(1)}, u32[]{:S(2)}, u32[]{:S(2)}) collective-permute-start(f16[128,4096]{1,0:T(8,128)(2,1)} %get-tuple-element.28), channel_id=1, source_target_pairs={{0,2},{2,0},{1,3},{3,1},{4,6},{6,4},{5,7},{7,5},{8,10},{10,8},{9,1... | collective-permute-start | bytes 3145736 | tf_op jit(solution)/shard_map/ppermute | solution.py:87
  94.5 38.9 %all-to-all-start = ((bf16[16,8,256]{2,1,0:T(8,128)(2,1)}), bf16[16,8,256]{2,1,0:T(8,128)(2,1)S(1)}, u32[]{:S(2)}, u32[]{:S(2)}) async-start(bf16[16,8,256]{2,1,0:T(8,128)(2,1)} %pad_maximum_fusion.6), calls=%async_computation | async-start | bytes 131072 | tf_op jit(solution)/shard_map/all_to_all | solution.py:181
  147.6 2.9 copy-start.7
  147.6 2.9 copy-start.14
  148.7 2.9 copy-start.3
  150.5 9.7 %collective-permute-start.3 = (f16[2,128,4096]{2,1,0:T(8,128)(2,1)}, f16[2,128,4096]{2,1,0:T(8,128)(2,1)}, u32[]{:S(2)}, u32[]{:S(2)}) collective-permute-start(f16[2,128,4096]{2,1,0:T(8,128)(2,1)} %pad_maximum_fusion), channel_id=1, source_target_pairs={{0,1},{1,0},{2,3},{3,2},{4,5},{5,4},{6,7},{7,6},{8,9},{9,8},{10,11... | collective-permute-start | bytes 6291464 | tf_op jit(solution)/shard_map/ppermute | solution.py:87
  153.2 2.0 copy-start.1
  153.2 2.2 copy-start.10
  159.5 4.5 %copy-start.5 = (bf16[8,2048]{1,0:T(8,128)(2,1)S(1)}, bf16[8,2048]{1,0:T(8,128)(2,1)}, u32[]{:S(2)}) copy-start(bf16[8,2048]{1,0:T(8,128)(2,1)} %param.24) | copy-start | bytes 98308
  159.9 5.4 %copy-start.8 = (f32[2048]{0:T(1024)S(1)}, f32[2048]{0:T(1024)}, u32[]{:S(2)}) copy-start(f32[2048]{0:T(1024)} %convert_element_type.262) | copy-start | bytes 24580
  159.9 5.5 %copy-start.6 = (f16[32,256]{1,0:T(8,128)(2,1)S(1)}, f16[32,256]{1,0:T(8,128)(2,1)}, u32[]{:S(2)}) copy-start(f16[32,256]{1,0:T(8,128)(2,1)} %convert_bitcast_fusion) | copy-start | bytes 49156
  162.7 7.7 %slice-start = ((f16[128,6272]{1,0:T(8,128)(2,1)}), f16[128,128]{1,0:T(8,128)(2,1)S(1)}, s32[]{:S(2)}) async-start(f16[128,6272]{1,0:T(8,128)(2,1)} %copy-done.2), calls=%async_computation.5 | async-start | bytes 65536 | tf_op jit(solution)/shard_map/slice | solution.py:168
  166.4 74.3 %all-to-all-start.1 = ((f16[8,32,1280]{2,1,0:T(8,128)(2,1)}), f16[8,32,1280]{2,1,0:T(8,128)(2,1)S(1)}, u32[]{:S(2)}, u32[]{:S(2)}) async-start(f16[8,32,1280]{2,1,0:T(8,128)(2,1)} %stack.41), calls=%async_computation.1 | async-start | bytes 1310720 | tf_op jit(solution)/shard_map/all_to_all | solution.py:20
  241.8 37.6 %all-to-all-start.2 = ((bf16[8,16,2048]{2,1,0:T(8,128)(2,1)}), bf16[8,16,2048]{2,1,0:T(8,128)(2,1)S(1)}, u32[]{:S(2)}, u32[]{:S(2)}) async-start(bf16[8,16,2048]{2,1,0:T(8,128)(2,1)} %bitcast.43), calls=%async_computation.2 | async-start | bytes 1048576 | tf_op jit(solution)/shard_map/all_to_all | solution.py:256
  250.9 28.6 %collective-permute-start.4 = (f16[256,768]{1,0:T(8,128)(2,1)S(1)}, f16[256,768]{1,0:T(8,128)(2,1)S(1)}, u32[]{:S(2)}, u32[]{:S(2)}) collective-permute-start(f16[256,768]{1,0:T(8,128)(2,1)S(1)} %get-tuple-element.32), channel_id=1, source_target_pairs={{0,4},{4,0},{1,5},{5,1},{2,6},{6,2},{3,7},{7,3},{8,12},{12,8},{9,1... | collective-permute-start | bytes 1179656 | tf_op jit(solution)/shard_map/ppermute | solution.py:87
  283.8 33.8 %all-to-all-start.3 = ((bf16[8,16,2048]{2,1,0:T(8,128)(2,1)}), bf16[8,16,2048]{2,1,0:T(8,128)(2,1)S(1)}, u32[]{:S(2)}, u32[]{:S(2)}) async-start(bf16[8,16,2048]{2,1,0:T(8,128)(2,1)} %bitcast.48), calls=%async_computation.3 | async-start | bytes 1048576 | tf_op jit(solution)/shard_map/all_to_all | solution.py:266
  291.8 25.8 %collective-permute-start.5 = (f16[2,256,768]{2,1,0:T(8,128)(2,1)S(1)}, f16[2,256,768]{2,1,0:T(8,128)(2,1)S(1)}, u32[]{:S(2)}, u32[]{:S(2)}) collective-permute-start(f16[2,256,768]{2,1,0:T(8,128)(2,1)S(1)} %get-tuple-element.30), channel_id=1, source_target_pairs={{0,2},{2,0},{1,3},{3,1},{4,6},{6,4},{5,7},{7,5},{8,10},{10,8},{9,1... | collective-permute-start | bytes 2359304 | tf_op jit(solution)/shard_map/ppermute | solution.py:87
  317.7 0.9 copy-start.4
  320.3 9.1 %collective-permute-start.6 = (f16[2,2,256,768]{3,2,1,0:T(8,128)(2,1)S(1)}, f16[2,2,256,768]{3,2,1,0:T(8,128)(2,1)}, u32[]{:S(2)}, u32[]{:S(2)}) collective-permute-start(f16[2,2,256,768]{3,2,1,0:T(8,128)(2,1)S(1)} %pad_maximum_fusion.1), channel_id=1, source_target_pairs={{0,1},{1,0},{2,3},{3,2},{4,5},{5,4},{6,7},{7,6},{8,9},{9,8},{10,11... | collective-permute-start | bytes 4718600 | tf_op jit(solution)/shard_map/ppermute | solution.py:87
  324.9 45.1 %all-to-all-start.4 = ((bf16[8,8,2048]{2,1,0:T(8,128)(2,1)}), bf16[8,8,2048]{2,1,0:T(8,128)(2,1)S(1)}, u32[]{:S(2)}, u32[]{:S(2)}) async-start(bf16[8,8,2048]{2,1,0:T(8,128)(2,1)} %fusion.1), calls=%async_computation.4 | async-start | bytes 524288 | tf_op jit(solution)/shard_map/all_to_all | solution.py:275
